TPU v7x, 512 devices: a whole 4x8x8 slice. The times are simulated.
512 devices in a mesh: ep: 32 (over z, x), tp: 16 (over y, core).
Axes of the slice: x: 4, y: 8, z: 8, core: 2. Of those that a mesh axis runs over, the one named last changes fastest.
Arguments:
- mixer_input: bfloat16 [4096, 2048], P('ep'), may hold values from -6 to 6
- mixer_gain: float32 [2048], replicated, may hold values from 0.1 to 1.9
- outer_weight: bfloat16 [2048, 1024], P(None, 'tp'), may hold values from -0.125 to 0.125
- inner_weight: bfloat16 [2048, 1024], P(None, 'tp'), may hold values from -0.125 to 0.125
- value_weight: bfloat16 [2048, 1024], P(None, 'tp'), may hold values from -0.125 to 0.125
- conv_kernel: bfloat16 [3, 1024], P(None, 'tp'), may hold values from -3 to 3
- group_gain: float32 [1024], P('tp'), may hold values from 0.1 to 1.9
- mixer_out_weight: bfloat16 [1024, 2048], P(None, 'tp'), may hold values from -0.1875 to 0.1875
- expert_input: bfloat16 [8192, 2048], P('ep'), may hold values from -6 to 6
- expert_gain: float32 [2048], replicated, may hold values from 0.1 to 1.9
- routes: int32 [8192, 2], P('ep'), may hold values from 0 to 31, all different within a row; in each aligned block of 256 rows (0 to 255, 256 to 511, ...) at most 32 rows name the same one
- route_weight: float32 [8192, 2], P('ep'), may hold values from 0.1 to 1
- expert_gate: bfloat16 [32, 2048, 3584], P('ep', None, 'tp'), may hold values from -0.125 to 0.125
- expert_up: bfloat16 [32, 2048, 3584], P('ep', None, 'tp'), may hold values from -0.125 to 0.125
- expert_down: bfloat16 [32, 3584, 2048], P('ep', None, 'tp'), may hold values from -0.09375 to 0.09375
Outputs:
- mixed_tokens: bfloat16 [4096, 2048], P('ep', 'tp')
- expert_tokens: bfloat16 [8192, 2048], P('ep', 'tp')
Inputs may be any that keep to these rules, and one draw needn't show every extreme that they name: `routes`: each row names 2 different experts. Within the rows of one index of ep no expert is named by more than 32 rows, a bound that some block reaches of them.
All inputs are finite; a program needn't handle non-finite values.
Results may differ from a plain program's by a relative error of at most 0.014.
Values may be sent and summed in bfloat16 or wider, within the bound.
A program may use at most 64 MiB of HBM per device.

v0:
```python
import jax
import jax.numpy as jnp
from jax import lax
from jax.sharding import PartitionSpec as P

GROUP = 64
EPS = 1e-06


def from_behind(block, axis, distance):
    devices = range(lax.axis_size(axis))
    route = [(i - distance, i) for i in devices if i - distance in devices]
    return lax.ppermute(block, axis, route)


def laid_out(tiles, dim):
    tiles = jnp.moveaxis(tiles, 0, dim)
    lengths = tiles.shape
    return tiles.reshape(*lengths[:dim], lengths[dim] * lengths[dim + 1], *lengths[dim + 2 :])


def sent_to_all(value, axis):
    size = lax.axis_size(axis)
    return lax.all_to_all(
        jnp.broadcast_to(value[None], (size, *value.shape)), axis, 0, 0, tiled=True
    )


def collect(value, axis, dim):
    return laid_out(sent_to_all(value, axis), dim)


def rms_scale(values, gain):
    floats = values.astype(jnp.float32)
    scale = lax.rsqrt(jnp.mean(floats * floats, axis=-1, keepdims=True) + EPS)
    return floats * scale * gain


def per_device(
    mixer_input,
    mixer_gain,
    outer_weight,
    inner_weight,
    value_weight,
    conv_kernel,
    group_gain,
    mixer_out_weight,
    expert_input,
    expert_gain,
    routes,
    route_weight,
    expert_gate,
    expert_up,
    expert_down,
):
    mix_count = mixer_input.shape[0]
    normed_a = rms_scale(mixer_input, mixer_gain).astype(jnp.bfloat16)
    outer = jnp.dot(normed_a, outer_weight, preferred_element_type=jnp.float32).astype(jnp.bfloat16)
    inner = jnp.dot(normed_a, inner_weight, preferred_element_type=jnp.float32).astype(jnp.bfloat16)
    values = jnp.dot(normed_a, value_weight, preferred_element_type=jnp.float32).astype(
        jnp.bfloat16
    )
    product = inner.astype(jnp.float32) * values.astype(jnp.float32)
    earlier_rows = from_behind(product[mix_count - 2 :], "ep", 1)
    padded = jnp.concatenate([earlier_rows, product], axis=0)
    kernel = conv_kernel.astype(jnp.float32)
    conv_sum = (
        kernel[0] * padded[0:mix_count]
        + kernel[1] * padded[1 : mix_count + 1]
        + kernel[2] * padded[2 : mix_count + 2]
    )
    gated = outer.astype(jnp.float32) * conv_sum
    grouped = gated.reshape(mix_count, -1, GROUP)
    grouped = rms_scale(grouped, group_gain.reshape(-1, GROUP))
    grouped = grouped.reshape(mix_count, -1).astype(jnp.bfloat16)
    weight_rows = mixer_out_weight
    mixed_tokens = jnp.dot(
        collect(grouped, "tp", 1), weight_rows, preferred_element_type=jnp.float32
    ).astype(jnp.bfloat16)
    exp_count, picks_each = routes.shape
    width = expert_input.shape[1]
    experts = expert_gate.shape[0] * lax.axis_size("ep")
    capacity = 2 * picks_each * exp_count // experts
    normed_b = rms_scale(expert_input, expert_gain).astype(jnp.bfloat16)
    picks = routes.reshape(-1)
    onehot = (picks[:, None] == jnp.arange(experts, dtype=jnp.int32)[None, :]).astype(jnp.int32)
    rank = jnp.sum((jnp.cumsum(onehot, axis=0) - onehot) * onehot, axis=1)
    slot = picks * capacity + rank
    token = jnp.arange(exp_count * picks_each, dtype=jnp.int32) // picks_each
    table = jnp.zeros((experts * capacity,), jnp.int32).at[slot].set(token + 1)
    valid = table > 0
    gathered_rows = jnp.take(normed_b, jnp.maximum(table - 1, 0), axis=0)
    buffer = jnp.where(valid[:, None], gathered_rows, 0).reshape(experts, capacity, width)
    gate_weight = expert_gate[0]
    up_weight = expert_up[0]
    down_weight = expert_down[0]
    out_cols = down_weight.shape[1]
    span = width // lax.axis_size("tp")
    outgoing = lax.dynamic_slice_in_dim(buffer, lax.axis_index("tp") * span, span, 2)
    received = lax.all_to_all(outgoing, "ep", split_axis=0, concat_axis=0, tiled=True)
    sources = received.shape[0]
    count = received.shape[1]
    piece = lax.all_gather(received, "tp", axis=2, tiled=True)
    span = piece.shape[2]
    flat_piece = piece.reshape(sources * count, span)
    gate = jnp.dot(flat_piece, gate_weight, preferred_element_type=jnp.float32)
    up_value = jnp.dot(flat_piece, up_weight, preferred_element_type=jnp.float32)
    hidden = (jax.nn.silu(gate) * up_value).astype(jnp.bfloat16)
    weight_rows = down_weight
    results = jnp.dot(
        lax.all_gather(hidden, "tp", axis=1, tiled=True),
        weight_rows,
        preferred_element_type=jnp.float32,
    ).astype(jnp.bfloat16)
    returned = lax.all_to_all(
        results.reshape(sources, count, out_cols), "ep", split_axis=0, concat_axis=0, tiled=True
    )
    flat_returned = returned.reshape(experts * capacity, out_cols)
    chosen = (
        jnp.take(flat_returned, slot, axis=0)
        .astype(jnp.float32)
        .reshape(exp_count, picks_each, out_cols)
    )
    weighted = jnp.sum(chosen * route_weight[..., None], axis=1)
    expert_tokens = weighted.astype(jnp.bfloat16)
    return (mixed_tokens, expert_tokens)


def solution(mesh):
    placed = (
        P("ep", None),
        P(),
        P(None, "tp"),
        P(None, "tp"),
        P(None, "tp"),
        P(None, "tp"),
        P("tp"),
        P(None, "tp"),
        P("ep", None),
        P(),
        P("ep", None),
        P("ep", None),
        P("ep", None, "tp"),
        P("ep", None, "tp"),
        P("ep", None, "tp"),
    )
    return jax.shard_map(
        per_device,
        mesh=mesh,
        in_specs=placed,
        out_specs=(P("ep", "tp"), P("ep", "tp")),
        check_vma=False,
    )
```

profile of v0, /device:TPU:24, one launch (start us, length us, event | category | flops | bytes accessed | tf_op | source)
XLA Modules:
  0.0 200.4 jit_solution(5589004506806771158)
XLA Ops:
  7.2 0.9 copy.25
  8.4 0.7 broadcast_multiply_fusion
  9.1 1.2 reduce-window.6
  11.0 2.4 %scatter_custom_fusion = s32[1024]{0:T(1024)S(1)} fusion(s32[512]{0:T(512)S(1)} %bitcast.57, s32[512]{0:T(512)S(1)} %fusion.28, s32[]{:T(128)} %constant.74.clone.1), kind=kCustom, calls=%fused_computation.67 | custom fusion | bytes 4100 | tf_op jit(solution)/shard_map/scatter | solution.py:90
  13.6 1.5 fusion
  15.1 1.5 fusion.2
  16.7 6.0 %gather_fusion = bf16[1024,2048]{1,0:T(8,128)(2,1)} fusion(bf16[256,2048]{1,0:T(8,128)(2,1)S(1)} %fusion.2, s32[1024]{0:T(1024)S(1)} %fusion.26), kind=kCustom, calls=%fused_computation | custom fusion | bytes 8392704 | tf_op jit(solution)/shard_map/jit(_take)/gather | solution.py:92
  22.6 1.4 fusion.15
  24.0 25.9 %all_to_all.15 = bf16[32,32,128]{2,1,0:T(8,128)(2,1)} all-to-all(bf16[32,32,128]{2,1,0:T(8,128)(2,1)S(1)} %fusion.15), channel_id=1, replica_groups=mesh['ep'=32,'tp'=16] {'ep'}, dimensions={0} | all-to-all | bytes 524288 | tf_op jit(solution)/shard_map/all_to_all | solution.py:100
  50.0 45.5 %all-gather.3.cloned.1.call-done = bf16[32,32,2048]{2,1,0:T(8,128)(2,1)} async-done(((bf16[32,32,128]{2,1,0:T(8,128)(2,1)}), bf16[32,32,2048]{2,1,0:T(8,128)(2,1)}) %all-gather.3.cloned.1.call-update) | async-done | bytes 4194320 | tf_op jit(solution)/shard_map/all_gather | solution.py:103
  95.5 3.7 %fusion.13 = f32[1024,224]{0,1:T(8,128)S(1)} fusion(bf16[1024,2048]{1,0:T(8,128)(2,1)} %bitcast.59, bf16[1,2048,224]{1,2,0:T(8,128)(2,1)S(1)} %copy-done), kind=kOutput, calls=%fused_computation.26 | convolution fusion | flops 939524096 | bytes 6029312 | tf_op jit(solution)/shard_map/dot_general | solution.py:106
  99.3 2.3 %fusion.3 = bf16[1024,224]{0,1:T(8,128)(2,1)} fusion(bf16[1024,2048]{1,0:T(8,128)(2,1)S(1)} %bitcast.60, bf16[1,2048,224]{1,2,0:T(8,128)(2,1)S(1)} %copy-done.8, f32[1024,224]{0,1:T(8,128)S(1)} %fusion.13), kind=kOutput, calls=%fused_computation.11 | convolution fusion | flops 940900352 | bytes 6488064 | tf_op jit(solution)/shard_map/dot_general | solution.py:107
  102.6 3.4 %collective-permute-start = (f32[2,64]{0,1:T(8,128)S(1)}, f32[2,64]{0,1:T(8,128)S(1)}, u32[]{:S(2)}, u32[]{:S(2)}) collective-permute-start(f32[2,64]{0,1:T(8,128)S(1)} %slice.36), channel_id=1, source_target_pairs={{0,16},{16,32},{32,48},{48,64},{64,80},{80,96},{96,112},{112,128},... | collective-permute-start | bytes 1544 | tf_op jit(solution)/shard_map/ppermute | solution.py:13
  106.3 1.3 collective-permute-done
  107.6 0.4 multiply_reduce_fusion.1
  108.1 0.8 broadcast_in_dim.53
  108.9 6.2 %all-to-all-start = ((bf16[16,128,64]{1,2,0:T(8,128)(2,1)}), bf16[16,128,64]{1,2,0:T(8,128)(2,1)S(1)}, u32[]{:S(2)}, u32[]{:S(2)}) async-start(bf16[16,128,64]{1,2,0:T(8,128)(2,1)} %broadcast_in_dim.53), calls=%async_computation | async-start | bytes 524288 | tf_op jit(solution)/shard_map/all_to_all | solution.py:24
  115.0 45.4 %all-gather.5.cloned.1.call-done = bf16[1024,3584]{0,1:T(8,128)(2,1)} async-done(((bf16[1024,224]{0,1:T(8,128)(2,1)}), bf16[1024,3584]{0,1:T(8,128)(2,1)}) %all-gather.5.cloned.1.call-update) | async-done | bytes 7340048 | tf_op jit(solution)/shard_map/all_gather | solution.py:111
  160.5 5.9 %convolution_convert_fusion = bf16[1024,128]{1,0:T(8,128)(2,1)} fusion(bf16[1024,3584]{0,1:T(8,128)(2,1)} %all-gather.5.cloned.1.call-done, bf16[1,3584,128]{2,1,0:T(8,128)(2,1)S(1)} %copy-done.9), kind=kOutput, calls=%fused_computation.12 | convolution fusion | flops 939655168 | bytes 8519680 | tf_op jit(solution)/shard_map/dot_general | solution.py:110
  166.4 10.3 %all-to-all-start.2 = ((bf16[32,32,128]{2,1,0:T(8,128)(2,1)}), bf16[32,32,128]{2,1,0:T(8,128)(2,1)S(1)}, u32[]{:S(2)}, u32[]{:S(2)}) async-start(bf16[32,32,128]{2,1,0:T(8,128)(2,1)} %bitcast.13), calls=%async_computation.2 | async-start | bytes 524288 | tf_op jit(solution)/shard_map/all_to_all | solution.py:115
  177.1 0.9 convolution_convert_fusion.1
  178.0 12.1 %all-to-all-done.2 = bf16[32,32,128]{2,1,0:T(8,128)(2,1)S(1)} async-done(((bf16[32,32,128]{2,1,0:T(8,128)(2,1)}), bf16[32,32,128]{2,1,0:T(8,128)(2,1)S(1)}, u32[]{:S(2)}, u32[]{:S(2)}) %all-to-all-start.2) | async-done | bytes 262176 | tf_op jit(solution)/shard_map/all_to_all | solution.py:115
  190.1 1.3 gather_fusion.1
  191.4 2.1 %multiply_reduce_fusion = bf16[256,128]{1,0:T(8,128)(2,1)} fusion(bf16[256,2,128]{2,1,0:T(2,128)(2,1)S(1)} %bitcast.55, pred[256,2]{1,0:T(8,128)(4,1)S(1)} %copy.29, f32[256,2]{1,0:T(8,128)S(1)} %copy.31), kind=kLoop, calls=%fused_computation.30 | loop fusion | flops 229376 | bytes 199168 | tf_op jit(solution)/shard_map/reduce_sum | solution.py:124
  (64 shorter events, 3.0 us)
Async XLA Ops:
  7.2 88.3 %copy-start = (bf16[1,2048,224]{1,2,0:T(8,128)(2,1)S(1)}, bf16[1,2048,224]{1,2,0:T(8,128)(2,1)}, u32[]{:S(2)}) copy-start(bf16[1,2048,224]{1,2,0:T(8,128)(2,1)} %param.27) | copy-start | bytes 2752516
  7.2 88.3 %all-gather.3.cloned.1.call-start = ((), (), s32[]{:S(2)}) async-start(), calls=%async_computation.3 | async-start | bytes 4456448 | tf_op jit(solution)/shard_map/all_gather | solution.py:103
  22.6 76.6 %copy-start.8 = (bf16[1,2048,224]{1,2,0:T(8,128)(2,1)S(1)}, bf16[1,2048,224]{1,2,0:T(8,128)(2,1)}, u32[]{:S(2)}) copy-start(bf16[1,2048,224]{1,2,0:T(8,128)(2,1)} %param.28) | copy-start | bytes 2752516
  49.9 110.5 %all-gather.5.cloned.1.call-start = ((), (), s32[]{:S(2)}) async-start(), calls=%async_computation.4 | async-start | bytes 7798784 | tf_op jit(solution)/shard_map/all_gather | solution.py:111
  95.5 3.7 %copy-start.7 = (bf16[32,32,2048]{2,1,0:T(8,128)(2,1)S(1)}, bf16[32,32,2048]{2,1,0:T(8,128)(2,1)}, u32[]{:S(2)}) copy-start(bf16[32,32,2048]{2,1,0:T(8,128)(2,1)} %all-gather.3.cloned.1.call-done) | copy-start | bytes 12582916
  99.2 2.4 %copy-start.1 = (bf16[128,2048]{1,0:T(8,128)(2,1)S(1)}, bf16[128,2048]{1,0:T(8,128)(2,1)}, u32[]{:S(2)}) copy-start(bf16[128,2048]{1,0:T(8,128)(2,1)} %param.15) | copy-start | bytes 1572868
  99.2 2.6 %copy-start.10 = (bf16[2048,64]{0,1:T(8,128)(2,1)S(1)}, bf16[2048,64]{0,1:T(8,128)(2,1)}, u32[]{:S(2)}) copy-start(bf16[2048,64]{0,1:T(8,128)(2,1)} %param.18) | copy-start | bytes 786436
  99.3 2.6 %copy-start.13 = (f32[2048]{0:T(1024)S(1)}, f32[2048]{0:T(1024)}, u32[]{:S(2)}) copy-start(f32[2048]{0:T(1024)} %param.16) | copy-start | bytes 24580
  99.3 2.9 %copy-start.11 = (bf16[2048,64]{0,1:T(8,128)(2,1)S(1)}, bf16[2048,64]{0,1:T(8,128)(2,1)}, u32[]{:S(2)}) copy-start(bf16[2048,64]{0,1:T(8,128)(2,1)} %param.19) | copy-start | bytes 786436
  99.3 6.8 %copy-start.5 = (bf16[3,64]{1,0:T(4,128)(2,1)S(1)}, bf16[3,64]{1,0:T(4,128)(2,1)}, u32[]{:S(2)}) copy-start(bf16[3,64]{1,0:T(4,128)(2,1)} %param.20) | copy-start | bytes 1156
  99.3 8.3 %copy-start.12 = (bf16[2048,64]{0,1:T(8,128)(2,1)S(1)}, bf16[2048,64]{0,1:T(8,128)(2,1)}, u32[]{:S(2)}) copy-start(bf16[2048,64]{0,1:T(8,128)(2,1)} %param.17) | copy-start | bytes 786436
  101.6 6.5 %copy-start.6 = (f32[64]{0:T(128)S(1)}, f32[64]{0:T(128)}, u32[]{:S(2)}) copy-start(f32[64]{0:T(128)} %param.21) | copy-start | bytes 772
  101.6 58.9 %copy-start.9 = (bf16[1,3584,128]{2,1,0:T(8,128)(2,1)S(1)}, bf16[1,3584,128]{2,1,0:T(8,128)(2,1)}, u32[]{:S(2)}) copy-start(bf16[1,3584,128]{2,1,0:T(8,128)(2,1)} %param.29) | copy-start | bytes 2752516
  102.6 5.0 %collective-permute-start = (f32[2,64]{0,1:T(8,128)S(1)}, f32[2,64]{0,1:T(8,128)S(1)}, u32[]{:S(2)}, u32[]{:S(2)}) collective-permute-start(f32[2,64]{0,1:T(8,128)S(1)} %slice.36), channel_id=1, source_target_pairs={{0,16},{16,32},{32,48},{48,64},{64,80},{80,96},{96,112},{112,128},... | collective-permute-start | bytes 1544 | tf_op jit(solution)/shard_map/ppermute | solution.py:13
  108.9 57.5 %all-to-all-start = ((bf16[16,128,64]{1,2,0:T(8,128)(2,1)}), bf16[16,128,64]{1,2,0:T(8,128)(2,1)S(1)}, u32[]{:S(2)}, u32[]{:S(2)}) async-start(bf16[16,128,64]{1,2,0:T(8,128)(2,1)} %broadcast_in_dim.53), calls=%async_computation | async-start | bytes 524288 | tf_op jit(solution)/shard_map/all_to_all | solution.py:24
  115.0 61.7 %copy-start.3 = (s32[256,2]{0,1:T(2,128)S(1)}, s32[256,2]{0,1:T(2,128)}, u32[]{:S(2)}) copy-start(s32[256,2]{0,1:T(2,128)} %param.25) | copy-start | bytes 6148
  115.0 61.9 %copy-start.4 = (f32[256,2]{0,1:T(2,128)S(1)}, f32[256,2]{0,1:T(2,128)}, u32[]{:S(2)}) copy-start(f32[256,2]{0,1:T(2,128)} %param.26) | copy-start | bytes 6148
  115.0 62.1 %copy-start.2 = (bf16[1024,128]{1,0:T(8,128)(2,1)S(1)}, bf16[1024,128]{1,0:T(8,128)(2,1)}, u32[]{:S(2)}) copy-start(bf16[1024,128]{1,0:T(8,128)(2,1)} %param.22) | copy-start | bytes 786436
  166.4 23.7 %all-to-all-start.2 = ((bf16[32,32,128]{2,1,0:T(8,128)(2,1)}), bf16[32,32,128]{2,1,0:T(8,128)(2,1)S(1)}, u32[]{:S(2)}, u32[]{:S(2)}) async-start(bf16[32,32,128]{2,1,0:T(8,128)(2,1)} %bitcast.13), calls=%async_computation.2 | async-start | bytes 524288 | tf_op jit(solution)/shard_map/all_to_all | solution.py:115
Sparse Core Ops, SparseCore 0:
  50.1 45.3 all-gather.2
  101.7 58.7 all-gather.4
where the time goes:
time: 201 us; the launch traced here: 200 us
  waiting for transfers between devices  104 us (52%)
  blocking collectives  25.9 us (13%)
  starting transfers between devices  19.9 us (10%)
  between operations  14.4 us (7%)
  matrix products  13.9 us (7%)
  local copies, waits for them, and re-layouts  13 us (6%)
  other arithmetic  8.83 us (4%)
    all_gather x1, waiting for transfers between devices, per_device(): piece = lax.all_gather(received, 'tp', axis=2, tiled=True)  45.5 us
    all_gather x1, waiting for transfers between devices, per_device(): lax.all_gather(hidden, 'tp', axis=1, tiled=True)  45.4 us
    all_to_all x1, blocking collectives, per_device(): lax.all_to_all(outgoing, 'ep', split_axis=0, concat_axis=0, tiled=True)  25.9 us
    all_to_all x1, waiting for transfers between devices, per_device(): lax.all_to_all(results.reshape(sources, count, out_cols), 'ep', split_axi...  12.1 us
    all_to_all x1, starting transfers between devices, per_device(): lax.all_to_all(results.reshape(sources, count, out_cols), 'ep', split_axi...  10.3 us
    all_to_all x1, starting transfers between devices, sent_to_all(): lax.all_to_all(jnp.broadcast_to(value[None], (size, *value.shape)), axis,...  6.16 us
    gather x1, local copies, waits for them, and re-layouts, per_device(): gathered_rows = jnp.take(normed_b, jnp.maximum(table - 1, 0), axis=0)  5.98 us
    dot_general x1, matrix products, per_device(): jnp.dot(lax.all_gather(hidden, 'tp', axis=1, tiled=True), weight_rows, pr...  5.92 us
  transfers between devices with their start and end apart: 5, of which 4 were waited for; matrix products, arithmetic and copies ran while one was open for 5% of the time, Pallas kernels for 0%

commit v1 on v0

--- a/solution.py
+++ b/solution.py
@@ -5,6 +5,13 @@
 
 GROUP = 64
 EPS = 1e-06
+
+
+def all_by_exchange(value, axis, dim):
+    size = lax.axis_size(axis)
+    parts = jnp.stack([value for _ in range(size)])
+    parts = lax.all_to_all(parts, axis, split_axis=0, concat_axis=0)
+    return jnp.concatenate(parts, axis=dim)
 
 
 def from_behind(block, axis, distance):
@@ -108,9 +115,7 @@
     hidden = (jax.nn.silu(gate) * up_value).astype(jnp.bfloat16)
     weight_rows = down_weight
     results = jnp.dot(
-        lax.all_gather(hidden, "tp", axis=1, tiled=True),
-        weight_rows,
-        preferred_element_type=jnp.float32,
+        all_by_exchange(hidden, "tp", 1), weight_rows, preferred_element_type=jnp.float32
     ).astype(jnp.bfloat16)
     returned = lax.all_to_all(
         results.reshape(sources, count, out_cols), "ep", split_axis=0, concat_axis=0, tiled=True

time: 201 us -> 324 us (1.61)
  the two profiles are of different devices: /device:TPU:24 before, /device:TPU:1 now
where the time goes in v1:
time: 324 us
  waiting for transfers between devices  224 us (69%)
  blocking collectives  24.9 us (8%)
  starting transfers between devices  21.4 us (7%)
  local copies, waits for them, and re-layouts  17 us (5%)
  between operations  14.4 us (4%)
  matrix products  13.2 us (4%)
  other arithmetic  8.83 us (3%)
    all_to_all x1, waiting for transfers between devices, all_by_exchange(): parts = lax.all_to_all(parts, axis, split_axis=0, concat_axis=0)  156 us
    all_gather x1, waiting for transfers between devices, per_device(): piece = lax.all_gather(received, 'tp', axis=2, tiled=True)  50.3 us
    all_to_all x1, blocking collectives, per_device(): lax.all_to_all(outgoing, 'ep', split_axis=0, concat_axis=0, tiled=True)  24.9 us
    all_to_all x1, waiting for transfers between devices, per_device(): lax.all_to_all(results.reshape(sources, count, out_cols), 'ep', split_axi...  11.1 us
    all_to_all x1, starting transfers between devices, per_device(): lax.all_to_all(results.reshape(sources, count, out_cols), 'ep', split_axi...  8.95 us
  transfers between devices with their start and end apart: 5, of which 5 were waited for; matrix products, arithmetic and copies ran while one was open for 3% of the time, Pallas kernels for 0%

profile of v1, /device:TPU:1, one launch (start us, length us, event | category | flops | bytes accessed | tf_op | source)
XLA Modules:
  0.0 323.8 jit_solution(12772069146382159846)
XLA Ops:
  7.2 0.9 copy.26
  9.1 1.2 reduce-window.6
  11.0 2.4 scatter_custom_fusion
  13.6 1.5 fusion
  15.1 1.5 fusion.2
  16.7 6.0 %gather_fusion = bf16[1024,2048]{1,0:T(8,128)(2,1)} fusion(bf16[256,2048]{1,0:T(8,128)(2,1)S(1)} %fusion.2, s32[1024]{0:T(1024)S(1)} %fusion.26), kind=kCustom, calls=%fused_computation | custom fusion | bytes 8392704 | tf_op jit(solution)/shard_map/jit(_take)/gather | solution.py:99
  22.6 1.4 fusion.15
  24.0 24.9 %all_to_all.20 = bf16[32,32,128]{2,1,0:T(8,128)(2,1)} all-to-all(bf16[32,32,128]{2,1,0:T(8,128)(2,1)S(1)} %fusion.15), channel_id=1, replica_groups=mesh['ep'=32,'tp'=16] {'ep'}, dimensions={0} | all-to-all | bytes 524288 | tf_op jit(solution)/shard_map/all_to_all | solution.py:107
  49.0 50.3 %all-gather.2.cloned.1.call-done = bf16[32,32,2048]{2,1,0:T(8,128)(2,1)} async-done(((bf16[32,32,128]{2,1,0:T(8,128)(2,1)}), bf16[32,32,2048]{2,1,0:T(8,128)(2,1)}) %all-gather.2.cloned.1.call-update) | async-done | bytes 4194320 | tf_op jit(solution)/shard_map/all_gather | solution.py:110
  99.3 3.7 %fusion.13 = f32[1024,224]{0,1:T(8,128)S(1)} fusion(bf16[1024,2048]{1,0:T(8,128)(2,1)} %bitcast.62, bf16[1,2048,224]{1,2,0:T(8,128)(2,1)S(1)} %copy-done), kind=kOutput, calls=%fused_computation.26 | convolution fusion | flops 939524096 | bytes 6029312 | tf_op jit(solution)/shard_map/dot_general | solution.py:113
  103.1 1.5 fusion.3
  104.6 4.0 %stack.2 = bf16[16,1024,224]{1,2,0:T(8,128)(2,1)} broadcast(bf16[1024,224]{0,1:T(8,128)(2,1)S(1)} %fusion.3), dimensions={1,2} | broadcast | bytes 7798784 | tf_op jit(solution)/shard_map/stack | solution.py:12
  108.6 4.8 %all-to-all-start.2 = ((bf16[16,1024,224]{1,2,0:T(8,128)(2,1)}), bf16[16,1024,224]{1,2,0:T(8,128)(2,1)}, u32[]{:S(2)}, u32[]{:S(2)}) async-start(bf16[16,1024,224]{1,2,0:T(8,128)(2,1)} %stack.2), calls=%async_computation.2 | async-start | bytes 14680064 | tf_op jit(solution)/shard_map/all_to_all | solution.py:13
  114.5 2.1 collective-permute-start
  116.9 0.8 collective-permute-done
  118.1 156.3 %all-to-all-done.2 = bf16[16,1024,224]{1,2,0:T(8,128)(2,1)} async-done(((bf16[16,1024,224]{1,2,0:T(8,128)(2,1)}), bf16[16,1024,224]{1,2,0:T(8,128)(2,1)}, u32[]{:S(2)}, u32[]{:S(2)}) %all-to-all-start.2) | async-done | bytes 7340064 | tf_op jit(solution)/shard_map/all_to_all | solution.py:13
  275.2 5.5 %all-to-all-start = ((bf16[16,128,64]{1,2,0:T(8,128)(2,1)}), bf16[16,128,64]{1,2,0:T(8,128)(2,1)S(1)}, u32[]{:S(2)}, u32[]{:S(2)}) async-start(bf16[16,128,64]{1,2,0:T(8,128)(2,1)} %broadcast_in_dim.53), calls=%async_computation | async-start | bytes 524288 | tf_op jit(solution)/shard_map/all_to_all | solution.py:31
  280.7 6.0 %convolution_convert_fusion = bf16[1024,128]{1,0:T(8,128)(2,1)} fusion(bf16[1024,3584]{0,1:T(8,128)(2,1)} %bitcast.13, bf16[1,3584,128]{2,1,0:T(8,128)(2,1)S(1)} %copy-done.9), kind=kOutput, calls=%fused_computation.12 | convolution fusion | flops 939655168 | bytes 8519680 | tf_op jit(solution)/shard_map/dot_general | solution.py:117
  286.7 5.6 %all-to-all-done = bf16[16,128,64]{1,2,0:T(8,128)(2,1)S(1)} async-done(((bf16[16,128,64]{1,2,0:T(8,128)(2,1)}), bf16[16,128,64]{1,2,0:T(8,128)(2,1)S(1)}, u32[]{:S(2)}, u32[]{:S(2)}) %all-to-all-start) | async-done | bytes 262176 | tf_op jit(solution)/shard_map/all_to_all | solution.py:31
  292.2 8.9 %all-to-all-start.3 = ((bf16[32,32,128]{2,1,0:T(8,128)(2,1)}), bf16[32,32,128]{2,1,0:T(8,128)(2,1)S(1)}, u32[]{:S(2)}, u32[]{:S(2)}) async-start(bf16[32,32,128]{2,1,0:T(8,128)(2,1)} %bitcast.15), calls=%async_computation.3 | async-start | bytes 524288 | tf_op jit(solution)/shard_map/all_to_all | solution.py:120
  301.6 0.9 convolution_convert_fusion.1
  302.5 11.1 %all-to-all-done.3 = bf16[32,32,128]{2,1,0:T(8,128)(2,1)S(1)} async-done(((bf16[32,32,128]{2,1,0:T(8,128)(2,1)}), bf16[32,32,128]{2,1,0:T(8,128)(2,1)S(1)}, u32[]{:S(2)}, u32[]{:S(2)}) %all-to-all-start.3) | async-done | bytes 262176 | tf_op jit(solution)/shard_map/all_to_all | solution.py:120
  313.5 1.3 gather_fusion.1
  314.9 2.1 multiply_reduce_fusion
  (64 shorter events, 4.7 us)
Async XLA Ops:
  7.2 92.1 %copy-start = (bf16[1,2048,224]{1,2,0:T(8,128)(2,1)S(1)}, bf16[1,2048,224]{1,2,0:T(8,128)(2,1)}, u32[]{:S(2)}) copy-start(bf16[1,2048,224]{1,2,0:T(8,128)(2,1)} %param.27) | copy-start | bytes 2752516
  7.2 92.1 %all-gather.2.cloned.1.call-start = ((), (), s32[]{:S(2)}) async-start(), calls=%async_computation.4 | async-start | bytes 4456448 | tf_op jit(solution)/shard_map/all_gather | solution.py:110
  22.6 80.4 %copy-start.8 = (bf16[1,2048,224]{1,2,0:T(8,128)(2,1)S(1)}, bf16[1,2048,224]{1,2,0:T(8,128)(2,1)}, u32[]{:S(2)}) copy-start(bf16[1,2048,224]{1,2,0:T(8,128)(2,1)} %param.28) | copy-start | bytes 2752516
  99.3 3.8 %copy-start.7 = (bf16[32,32,2048]{2,1,0:T(8,128)(2,1)S(1)}, bf16[32,32,2048]{2,1,0:T(8,128)(2,1)}, u32[]{:S(2)}) copy-start(bf16[32,32,2048]{2,1,0:T(8,128)(2,1)} %all-gather.2.cloned.1.call-done) | copy-start | bytes 12582916
  108.5 4.9 %copy-start.1 = (bf16[128,2048]{1,0:T(8,128)(2,1)S(1)}, bf16[128,2048]{1,0:T(8,128)(2,1)}, u32[]{:S(2)}) copy-start(bf16[128,2048]{1,0:T(8,128)(2,1)} %param.15) | copy-start | bytes 1572868
  108.5 5.1 %copy-start.10 = (bf16[2048,64]{0,1:T(8,128)(2,1)S(1)}, bf16[2048,64]{0,1:T(8,128)(2,1)}, u32[]{:S(2)}) copy-start(bf16[2048,64]{0,1:T(8,128)(2,1)} %param.18) | copy-start | bytes 786436
  108.5 5.1 %copy-start.13 = (f32[2048]{0:T(1024)S(1)}, f32[2048]{0:T(1024)}, u32[]{:S(2)}) copy-start(f32[2048]{0:T(1024)} %param.16) | copy-start | bytes 24580
  108.6 5.5 %copy-start.11 = (bf16[2048,64]{0,1:T(8,128)(2,1)S(1)}, bf16[2048,64]{0,1:T(8,128)(2,1)}, u32[]{:S(2)}) copy-start(bf16[2048,64]{0,1:T(8,128)(2,1)} %param.19) | copy-start | bytes 786436
  108.6 8.1 %copy-start.5 = (bf16[3,64]{1,0:T(4,128)(2,1)S(1)}, bf16[3,64]{1,0:T(4,128)(2,1)}, u32[]{:S(2)}) copy-start(bf16[3,64]{1,0:T(4,128)(2,1)} %param.20) | copy-start | bytes 1156
  108.6 9.1 %copy-start.12 = (bf16[2048,64]{0,1:T(8,128)(2,1)S(1)}, bf16[2048,64]{0,1:T(8,128)(2,1)}, u32[]{:S(2)}) copy-start(bf16[2048,64]{0,1:T(8,128)(2,1)} %param.17) | copy-start | bytes 786436
  108.6 165.8 %all-to-all-start.2 = ((bf16[16,1024,224]{1,2,0:T(8,128)(2,1)}), bf16[16,1024,224]{1,2,0:T(8,128)(2,1)}, u32[]{:S(2)}, u32[]{:S(2)}) async-start(bf16[16,1024,224]{1,2,0:T(8,128)(2,1)} %stack.2), calls=%async_computation.2 | async-start | bytes 14680064 | tf_op jit(solution)/shard_map/all_to_all | solution.py:13
  113.4 4.6 %copy-start.6 = (f32[64]{0:T(128)S(1)}, f32[64]{0:T(128)}, u32[]{:S(2)}) copy-start(f32[64]{0:T(128)} %param.21) | copy-start | bytes 772
  113.4 167.2 %copy-start.9 = (bf16[1,3584,128]{2,1,0:T(8,128)(2,1)S(1)}, bf16[1,3584,128]{2,1,0:T(8,128)(2,1)}, u32[]{:S(2)}) copy-start(bf16[1,3584,128]{2,1,0:T(8,128)(2,1)} %param.29) | copy-start | bytes 2752516
  114.5 3.1 collective-permute-start
  275.2 17.1 %all-to-all-start = ((bf16[16,128,64]{1,2,0:T(8,128)(2,1)}), bf16[16,128,64]{1,2,0:T(8,128)(2,1)S(1)}, u32[]{:S(2)}, u32[]{:S(2)}) async-start(bf16[16,128,64]{1,2,0:T(8,128)(2,1)} %broadcast_in_dim.53), calls=%async_computation | async-start | bytes 524288 | tf_op jit(solution)/shard_map/all_to_all | solution.py:31
  280.7 20.5 %copy-start.3 = (s32[256,2]{0,1:T(2,128)S(1)}, s32[256,2]{0,1:T(2,128)}, u32[]{:S(2)}) copy-start(s32[256,2]{0,1:T(2,128)} %param.25) | copy-start | bytes 6148
  280.7 20.7 %copy-start.4 = (f32[256,2]{0,1:T(2,128)S(1)}, f32[256,2]{0,1:T(2,128)}, u32[]{:S(2)}) copy-start(f32[256,2]{0,1:T(2,128)} %param.26) | copy-start | bytes 6148
  280.7 20.9 %copy-start.2 = (bf16[1024,128]{1,0:T(8,128)(2,1)S(1)}, bf16[1024,128]{1,0:T(8,128)(2,1)}, u32[]{:S(2)}) copy-start(bf16[1024,128]{1,0:T(8,128)(2,1)} %param.22) | copy-start | bytes 786436
  292.2 21.3 %all-to-all-start.3 = ((bf16[32,32,128]{2,1,0:T(8,128)(2,1)}), bf16[32,32,128]{2,1,0:T(8,128)(2,1)S(1)}, u32[]{:S(2)}, u32[]{:S(2)}) async-start(bf16[32,32,128]{2,1,0:T(8,128)(2,1)} %bitcast.15), calls=%async_computation.3 | async-start | bytes 524288 | tf_op jit(solution)/shard_map/all_to_all | solution.py:120
Sparse Core Ops, SparseCore 0:
  49.1 50.1 all-gather.1
